TPU v7x, 32 devices: a whole 2x2x4 slice. The times are simulated.
32 devices in a mesh: fs: 8 (over z, y), tp: 4 (over x, core).
Axes of the slice: x: 2, y: 2, z: 4, core: 2. Of those that a mesh axis runs over, the one named last changes fastest.
Arguments:
- resid: bfloat16 [12288, 2048], P(('fs', 'tp')), may hold values from -6 to 6
- norm1_gain: float32 [2048], replicated, may hold values from 0.1 to 1.9
- w_value: float32 [2048, 2048], P('fs', 'tp'), may hold values from -0.125 to 0.125
- w_gate: float32 [2048, 2048], P('fs', 'tp'), may hold values from -0.125 to 0.125
- value_scale: float32 [2048], replicated, may hold values from 0.3 to 3
- gate_scale: float32 [2048], replicated, may hold values from 0.5 to 3
- conv_taps: float32 [31, 2048], replicated, may hold values from -1 to 1
- conv_gain: float32 [2048], replicated, may hold values from 0.1 to 1.9
- w_point: float32 [2048, 2048], P('tp', 'fs'), may hold values from -0.125 to 0.125
- point_scale: float32 [2048], P('fs'), may hold values from 0.5 to 3
- norm2_gain: float32 [2048], replicated, may hold values from 0.1 to 1.9
- w_up: float32 [2048, 8192], P('fs', 'tp'), may hold values from -0.125 to 0.125
- up_scale: float32 [8192], P('tp'), may hold values from 0.5 to 1.5
- w_down: float32 [8192, 2048], P('tp', 'fs'), may hold values from -0.0625 to 0.0625
- down_scale: float32 [2048], P('fs'), may hold values from 0.3 to 1
Outputs:
- layer_out: bfloat16 [12288, 2048], P(('fs', 'tp'))
All inputs are finite; a program needn't handle non-finite values.
Results may differ from a plain program's by a relative error of at most 0.015.
Values may be sent and summed in bfloat16 or wider, within the bound.
A program may use at most 128 MiB of HBM per device.

v0:
```python
import jax
import jax.numpy as jnp
from jax import lax
from jax.sharding import PartitionSpec as P

GROUPS = 4


def rms_scaled(values, gain):
    data = values.astype(jnp.float32)
    return data * lax.rsqrt(jnp.mean(data * data, axis=-1, keepdims=True) + 1e-06) * gain


def depthwise(padded, taps, length):
    wide = padded.astype(jnp.float32)
    conv = jnp.zeros((length, wide.shape[1]), jnp.float32)
    for offset in range(taps.shape[0]):
        conv = conv + taps[offset] * wide[offset : offset + length]
    return conv


def fetch_mlp(up_bf, down_bf):
    return (
        lax.all_gather(up_bf, "fs", axis=0, tiled=True),
        lax.all_gather(down_bf, "fs", axis=1, tiled=True),
    )


def shards(
    resid,
    norm1_gain,
    w_value,
    w_gate,
    value_scale,
    gate_scale,
    conv_taps,
    conv_gain,
    w_point,
    point_scale,
    norm2_gain,
    w_up,
    up_scale,
    w_down,
    down_scale,
):
    tok_rows = resid.shape[0]
    tp_count = lax.axis_size("tp")
    tp_rank = lax.axis_index("tp")
    seq_len = tok_rows * tp_count
    channels = value_scale.shape[0]
    group_width = channels // GROUPS
    reach = conv_taps.shape[0] // 2
    value_bf = w_value.astype(jnp.bfloat16)
    gate_bf = w_gate.astype(jnp.bfloat16)
    point_bf = w_point.astype(jnp.bfloat16)
    up_bf = w_up.astype(jnp.bfloat16)
    down_bf = w_down.astype(jnp.bfloat16)
    point_full, down_full = (
        lax.all_gather(point_scale, "fs", axis=0, tiled=True),
        lax.all_gather(down_scale, "fs", axis=0, tiled=True),
    )
    normed = rms_scaled(resid, norm1_gain).astype(jnp.bfloat16)
    value_rows, gate_rows, point_rows = (
        lax.all_gather(value_bf, "fs", axis=0, tiled=True),
        lax.all_gather(gate_bf, "fs", axis=0, tiled=True),
        lax.all_gather(point_bf, "fs", axis=1, tiled=True),
    )
    own_width = value_rows.shape[1]
    first = tp_rank * own_width
    own_value_scale = lax.dynamic_slice_in_dim(value_scale, first, own_width, 0)
    own_gate_scale = lax.dynamic_slice_in_dim(gate_scale, first, own_width, 0)
    own_taps = lax.dynamic_slice_in_dim(conv_taps, first, own_width, 1)
    own_gain = lax.dynamic_slice_in_dim(conv_gain, first, own_width, 0)
    piece = lax.all_gather(normed, "tp", axis=0, tiled=True)
    value = jnp.dot(piece, value_rows, preferred_element_type=jnp.float32) * own_value_scale
    gate = jnp.dot(piece, gate_rows, preferred_element_type=jnp.float32) * own_gate_scale
    glu_seq = (value * jax.nn.sigmoid(gate)).astype(jnp.bfloat16)
    padded = jnp.pad(glu_seq, ((reach, reach), (0, 0)))
    conv = depthwise(padded, own_taps, seq_len)
    member = ((first + jnp.arange(own_width)) % GROUPS)[:, None] == jnp.arange(GROUPS)[None, :]
    member = member.astype(jnp.float32)
    sums = jnp.dot(conv, member, precision=lax.Precision.HIGHEST)
    squares = jnp.dot(conv * conv, member, precision=lax.Precision.HIGHEST)
    totals, square_totals = lax.psum((sums, squares), "tp")
    gmean = jnp.dot(totals / group_width, member.T, precision=lax.Precision.HIGHEST)
    gsquare = jnp.dot(square_totals / group_width, member.T, precision=lax.Precision.HIGHEST)
    scaled = (conv - gmean) * lax.rsqrt(gsquare - gmean * gmean + 1e-05) * own_gain
    act = jax.nn.silu(scaled).astype(jnp.bfloat16)
    mixed = lax.psum_scatter(
        jnp.dot(act, point_rows, preferred_element_type=jnp.float32) * point_full,
        "tp",
        scatter_dimension=0,
        tiled=True,
    )
    middle = (resid.astype(jnp.float32) + mixed).astype(jnp.bfloat16)
    normed2 = rms_scaled(middle, norm2_gain).astype(jnp.bfloat16)
    up_cols, down_part = fetch_mlp(up_bf, down_bf)
    upper = (
        jnp.dot(
            lax.all_gather(normed2, "tp", axis=0, tiled=True),
            up_cols,
            preferred_element_type=jnp.float32,
        )
        * up_scale
    )
    hidden = jnp.square(jax.nn.relu(upper)).astype(jnp.bfloat16)
    total = lax.psum_scatter(
        (jnp.dot(hidden, down_part, preferred_element_type=jnp.float32) * down_full).astype(
            jnp.bfloat16
        ),
        "tp",
        scatter_dimension=0,
        tiled=True,
    ).astype(jnp.float32)
    return (middle.astype(jnp.float32) + total).astype(jnp.bfloat16)


def solution(mesh):
    in_specs = (
        P(("fs", "tp"), None),
        P(),
        P("fs", "tp"),
        P("fs", "tp"),
        P(),
        P(),
        P(),
        P(),
        P("tp", "fs"),
        P("fs"),
        P(),
        P("fs", "tp"),
        P("tp"),
        P("tp", "fs"),
        P("fs"),
    )
    out_specs = P(("fs", "tp"), None)
    return jax.shard_map(shards, mesh=mesh, in_specs=in_specs, out_specs=out_specs, check_vma=False)
```

profile of v0, /device:TPU:0, one launch (start us, length us, event | category | flops | bytes accessed | tf_op | source)
XLA Modules:
  0.0 733.7 jit_solution(1871999571624865409)
XLA Ops:
  6.5 1.9 convert_element_type.59
  8.5 1.8 fusion.11
  10.4 2.3 fusion.13
  14.4 0.8 dynamic_slice.14
  16.7 22.4 %all-gather = f32[8,1,256]{2,1,0:T(1,128)S(1)} all-gather(f32[1,1,256]{2,1,0:T(1,128)S(1)} %bitcast.78), channel_id=1, replica_groups=mesh['fs'=8,'tp'=4] {'fs'}, dimensions={0}, use_global_device_ids=true | all-gather | bytes 9216 | tf_op jit(solution)/shard_map/all_gather | solution.py:59
  39.1 1.2 fusion.67
  40.3 1.4 constant_dynamic-slice_fusion
  41.7 19.7 %all-gather.14.cloned.1.call-done = bf16[2048,512]{1,0:T(8,128)(2,1)} async-done(((bf16[256,512]{1,0:T(8,128)(2,1)}), bf16[2048,512]{1,0:T(8,128)(2,1)}) %all-gather.14.cloned.1.call-update) | async-done | bytes 2097168 | tf_op jit(solution)/shard_map/all_gather | solution.py:65
  61.4 46.5 %all-gather.10.cloned.1.call-done = bf16[1536,2048]{1,0:T(8,128)(2,1)} async-done(((bf16[384,2048]{1,0:T(8,128)(2,1)}), bf16[1536,2048]{1,0:T(8,128)(2,1)}) %all-gather.10.cloned.1.call-update) | async-done | bytes 6291472 | tf_op jit(solution)/shard_map/all_gather | solution.py:74
  107.9 9.0 %fusion.10 = f32[1536,512]{1,0:T(8,128)} fusion(bf16[1536,2048]{1,0:T(8,128)(2,1)} %all-gather.10.cloned.1.call-done, bf16[2048,512]{1,0:T(8,128)(2,1)} %all-gather.14.cloned.1.call-done, f32[512]{0:T(512)S(1)} %dynamic_slice.14), kind=kOutput, calls=%fused_computation.22 | convolution fusion | flops 3224371200 | bytes 11536384 | tf_op jit(solution)/shard_map/dot_general | solution.py:76
  116.9 42.2 %all-gather.12.cloned.1.call-done = bf16[2048,512]{1,0:T(8,128)(2,1)} async-done(((bf16[256,512]{1,0:T(8,128)(2,1)}), bf16[2048,512]{1,0:T(8,128)(2,1)}) %all-gather.12.cloned.1.call-update) | async-done | bytes 2097168 | tf_op jit(solution)/shard_map/all_gather | solution.py:64
  159.1 7.8 %fusion.51 = bf16[1536,512]{1,0:T(8,128)(2,1)S(1)} fusion(f32[1536,512]{1,0:T(8,128)} %fusion.10, bf16[1536,2048]{1,0:T(8,128)(2,1)} %all-gather.10.cloned.1.call-done, bf16[2048,512]{1,0:T(8,128)(2,1)} %all-gather.12.cloned.1.call-done, f32[512]{0:T(512)S(1)} %dynamic_slice.13), kind=kOutput, calls=%fused_computation.95 | convolution fusion | flops 3223584768 | bytes 13109248 | tf_op jit(solution)/shard_map/dot_general | solution.py:75
  167.4 12.0 %fusion.19 = f32[1536,512]{1,0:T(8,128)S(1)} fusion(f32[1566,512]{1,0:T(8,128)S(1)} %pad_convert_fusion, f32[512]{0:T(512)S(1)} %bitcast.57, f32[512]{0:T(512)S(1)} %bitcast.59, f32[512]{0:T(512)S(1)} %bitcast.60, f32[512]{0:T(512)S(1)} %bitcast.61, f32[512]{0:T(512)S(1)} %bitcast.62, f32[512]{0:T(512)S(1)} %bitcast.63, f32[512]{0:T(512)S(1)} %bitcast.64, ...), kind=kLoop, calls=%fused_computation.32 | loop fusion | flops 47972352 | bytes 100726784 | tf_op jit(solution)/shard_map/add | solution.py:18
  179.4 2.6 fusion.49
  182.0 2.5 fusion.57
  184.5 33.5 %all-reduce.1 = (f32[1536,4]{1,0:T(8,128)}, f32[1536,4]{1,0:T(8,128)}) all-reduce(f32[1536,4]{1,0:T(8,128)} %fusion.57, f32[1536,4]{1,0:T(8,128)} %fusion.49), channel_id=1, replica_groups=mesh['fs'=8,'tp'=4] {'tp'}, use_global_device_ids=true, to_apply=%region_1.2 | all-reduce | flops 12288 | bytes 98304 | tf_op jit(solution)/shard_map/psum | solution.py:84
  218.0 2.7 fusion.53
  220.7 3.7 multiply_convert_fusion.2
  224.4 10.0 %convolution_multiply_fusion = f32[1536,2048]{1,0:T(8,128)} fusion(bf16[1536,512]{1,0:T(8,128)(2,1)} %multiply_convert_fusion.2, bf16[512,2048]{1,0:T(8,128)(2,1)} %all-gather.16.cloned.1.call-done, f32[2048]{0:T(1024)S(1)} %bitcast.76), kind=kOutput, calls=%fused_computation.2 | convolution fusion | flops 3224371200 | bytes 16261120 | tf_op jit(solution)/shard_map/dot_general | solution.py:90
  234.5 1.5 copy-done.2
  236.0 1.2 convert_element_type.67
  237.2 3.4 convert_element_type.69
  240.8 91.7 %reduce-scatter.3.cloned.1.call-done = f32[384,2048]{1,0:T(8,128)} async-done(((f32[1536,2048]{1,0:T(8,128)}), f32[384,2048]{1,0:T(8,128)}) %reduce-scatter.3.cloned.1.call-update) | async-done | bytes 3145744 | tf_op jit(solution)/shard_map/reduce_scatter | solution.py:89
  332.5 2.4 fusion.15
  334.9 1.6 fusion.17
  336.6 21.2 %all-gather.1 = f32[8,1,256]{2,1,0:T(1,128)S(1)} all-gather(f32[1,1,256]{2,1,0:T(1,128)S(1)} %bitcast.79), channel_id=1, replica_groups=mesh['fs'=8,'tp'=4] {'fs'}, dimensions={0}, use_global_device_ids=true | all-gather | bytes 9216 | tf_op jit(solution)/shard_map/all_gather | solution.py:60
  357.8 101.1 %all-gather.20.cloned.1.call-done = bf16[2048,2048]{1,0:T(8,128)(2,1)} async-done(((bf16[256,2048]{1,0:T(8,128)(2,1)}), bf16[2048,2048]{1,0:T(8,128)(2,1)}) %all-gather.20.cloned.1.call-update) | async-done | bytes 8388624 | tf_op jit(solution)/shard_map/all_gather | solution.py:24
  459.0 125.2 %all-gather.22.cloned.1.call-done = bf16[2048,2048]{1,0:T(8,128)(2,1)} async-done(((bf16[2048,256]{1,0:T(8,128)(2,1)}), bf16[2048,2048]{1,0:T(8,128)(2,1)}) %all-gather.22.cloned.1.call-update) | async-done | bytes 8388624 | tf_op jit(solution)/shard_map/all_gather | solution.py:25
  584.1 46.1 %all-gather.18.cloned.1.call-done = bf16[1536,2048]{1,0:T(8,128)(2,1)} async-done(((bf16[384,2048]{1,0:T(8,128)(2,1)}), bf16[1536,2048]{1,0:T(8,128)(2,1)}) %all-gather.18.cloned.1.call-update) | async-done | bytes 6291472 | tf_op jit(solution)/shard_map/all_gather | solution.py:100
  630.3 34.7 %multiply_convert_fusion = bf16[1536,2048]{1,0:T(8,128)(2,1)} fusion(bf16[2048,2048]{1,0:T(8,128)(2,1)} %all-gather.22.cloned.1.call-done, bf16[1536,2048]{1,0:T(8,128)(2,1)} %all-gather.18.cloned.1.call-done, bf16[2048,2048]{1,0:T(8,128)(2,1)} %all-gather.20.cloned.1.call-done, f32[2048]{0:T(1024)S(1)} %bitcast.77, f32[2048]{0:T(1024)S(1)} %copy-done.9), kind=kOutput, calls=%fused_computation | convolution fusion | flops 25788678144 | bytes 29376512 | tf_op jit(solution)/shard_map/dot_general | solution.py:108
  665.0 59.0 %reduce-scatter.5.cloned.1.call-done = bf16[384,2048]{1,0:T(8,128)(2,1)} async-done(((bf16[1536,2048]{1,0:T(8,128)(2,1)}), bf16[384,2048]{1,0:T(8,128)(2,1)}) %reduce-scatter.5.cloned.1.call-update) | async-done | bytes 1572880 | tf_op jit(solution)/shard_map/reduce_scatter | solution.py:107
  724.0 3.2 fusion.18
  (46 shorter events, 4.0 us)
Async XLA Ops:
  6.5 3.8 copy-start
  6.5 54.9 %all-gather.14.cloned.1.call-start = ((), (), s32[]{:S(2)}) async-start(), calls=%async_computation.4 | async-start | bytes 2359296 | tf_op jit(solution)/shard_map/all_gather | solution.py:65
  8.5 4.3 copy-start.3
  8.5 99.4 %all-gather.10.cloned.1.call-start = ((), (), s32[]{:S(2)}) async-start(), calls=%async_computation.2 | async-start | bytes 7864320 | tf_op jit(solution)/shard_map/all_gather | solution.py:74
  10.4 3.3 copy-start.4
  10.4 6.3 copy-start.6
  12.7 146.4 %all-gather.12.cloned.1.call-start = ((), (), s32[]{:S(2)}) async-start(), calls=%async_computation.3 | async-start | bytes 2359296 | tf_op jit(solution)/shard_map/all_gather | solution.py:64
  13.6 210.8 %all-gather.16.cloned.1.call-start = ((), (), s32[]{:S(2)}) async-start(), calls=%async_computation.5 | async-start | bytes 2359296 | tf_op jit(solution)/shard_map/all_gather | solution.py:66
  14.4 318.1 %reduce-scatter.3.cloned.1.call-start = ((), (), s32[]{:S(2)}) async-start(), calls=%async_computation.6 | async-start | bytes 15728640 | tf_op jit(solution)/shard_map/reduce_scatter | solution.py:89
  218.0 2.7 copy-start.8
  234.4 1.6 copy-start.2
  234.4 224.5 %all-gather.20.cloned.1.call-start = ((), (), s32[]{:S(2)}) async-start(), calls=%async_computation.8 | async-start | bytes 9437184 | tf_op jit(solution)/shard_map/all_gather | solution.py:24
  237.2 95.3 %copy-start.1 = (bf16[384,2048]{1,0:T(8,128)(2,1)S(1)}, bf16[384,2048]{1,0:T(8,128)(2,1)}, u32[]{:S(2)}) copy-start(bf16[384,2048]{1,0:T(8,128)(2,1)} %param.15) | copy-start | bytes 4718596
  237.2 346.9 %all-gather.22.cloned.1.call-start = ((), (), s32[]{:S(2)}) async-start(), calls=%async_computation.9 | async-start | bytes 9437184 | tf_op jit(solution)/shard_map/all_gather | solution.py:25
  240.7 94.2 %copy-start.5 = (f32[2048]{0:T(1024)S(1)}, f32[2048]{0:T(1024)}, u32[]{:S(2)}) copy-start(f32[2048]{0:T(1024)} %param.25) | copy-start | bytes 24580
  240.7 389.5 %all-gather.18.cloned.1.call-start = ((), (), s32[]{:S(2)}) async-start(), calls=%async_computation.7 | async-start | bytes 7864320 | tf_op jit(solution)/shard_map/all_gather | solution.py:100
  334.9 1.7 copy-start.7
  334.9 295.4 %copy-start.9 = (f32[2048]{0:T(1024)S(1)}, f32[2048]{0:T(1024)}, u32[]{:S(2)}) copy-start(f32[2048]{0:T(1024)} %param.27) | copy-start | bytes 24580
  336.5 387.4 %reduce-scatter.5.cloned.1.call-start = ((), (), s32[]{:S(2)}) async-start(), calls=%async_computation.10 | async-start | bytes 7864320 | tf_op jit(solution)/shard_map/reduce_scatter | solution.py:107
Sparse Core Ops, SparseCore 0:
  9.5 51.9 all-gather.13
  63.0 44.8 all-gather.9
  110.0 49.0 all-gather.11
  161.0 48.8 all-gather.15
  234.6 97.8 reduce-scatter.2
  334.5 124.4 all-gather.19
  461.0 123.0 all-gather.21
  585.7 44.5 all-gather.17
  665.1 58.8 reduce-scatter.4
where the time goes:
time: 734 us
  waiting for transfers between devices  532 us (72%)
  blocking collectives  77.1 us (11%)
  matrix products  73 us (10%)
  other arithmetic  31.7 us (4%)
  between operations  13.4 us (2%)
    all_gather x1, waiting for transfers between devices, fetch_mlp(): lax.all_gather(down_bf, 'fs', axis=1, tiled=True)  125 us
    all_gather x1, waiting for transfers between devices, fetch_mlp(): lax.all_gather(up_bf, 'fs', axis=0, tiled=True)  101 us
    reduce_scatter x1, waiting for transfers between devices, shards(): lax.psum_scatter(jnp.dot(act, point_rows, preferred_element_type=jnp.floa...  91.7 us
    reduce_scatter x1, waiting for transfers between devices, shards(): lax.psum_scatter((jnp.dot(hidden, down_part, preferred_element_type=jnp.f...  59 us
    all_gather x1, waiting for transfers between devices, shards(): piece = lax.all_gather(normed, 'tp', axis=0, tiled=True)  46.5 us
    all_gather x1, waiting for transfers between devices, shards(): lax.all_gather(normed2, 'tp', axis=0, tiled=True)  46.1 us
    all_gather x1, waiting for transfers between devices, shards(): lax.all_gather(value_bf, 'fs', axis=0, tiled=True)  42.2 us
    dot_general x1, matrix products, shards(): jnp.dot(hidden, down_part, preferred_element_type=jnp.float32) * down_full  34.7 us
  transfers between devices with their start and end apart: 9, of which 8 were waited for; matrix products, arithmetic and copies ran while one was open for 8% of the time, Pallas kernels for 0%

commit v1 on v0

v1 whole, which is shorter than its diff:
```python
import functools

import jax
import jax.numpy as jnp
from jax import lax
from jax.experimental import pallas as pl
from jax.experimental.pallas import tpu as pltpu
from jax.sharding import PartitionSpec as P


GROUPS = 4
CORES = 2
MESH = pl.DeviceIdType.MESH


def rms_scaled(values, gain):
    data = values.astype(jnp.float32)
    return data * lax.rsqrt(jnp.mean(data * data, axis=-1, keepdims=True) + 1e-06) * gain


def depthwise(padded, taps, length):
    wide = padded.astype(jnp.float32)
    conv = jnp.zeros((length, wide.shape[1]), jnp.float32)
    for offset in range(taps.shape[0]):
        conv = conv + taps[offset] * wide[offset : offset + length]
    return conv


def place(n):
    me = lax.axis_index("tp")
    core = lax.rem(me, CORES)
    chip = me // CORES
    chips = n // CORES
    partner = chip * CORES + (CORES - 1 - core)
    return me, core, chip, chips, partner


def chip_core(chip, core, chips):
    return lax.rem(chip + 2 * chips, chips) * CORES + core


def greet(core, chip, chips, partner):
    barrier = pltpu.get_barrier_semaphore()
    pl.semaphore_signal(barrier, inc=1, device_id={"tp": partner}, device_id_type=MESH)
    for d in range(1, chips):
        pl.semaphore_signal(
            barrier, inc=1, device_id={"tp": chip_core(chip + d, core, chips)}, device_id_type=MESH
        )
    pl.semaphore_wait(barrier, chips)


def gather_kernel(n, pieces, x_ref, out_ref, own_sem, far_send, far_recv, near_send, near_recv):
    me, core, chip, chips, partner = place(n)
    rows = x_ref.shape[0]
    step = rows // pieces
    greet(core, chip, chips, partner)

    def spot(owner, k):
        return out_ref.at[pl.ds(pl.multiple_of(owner * rows + k * step, step), step)]

    def src(k):
        return x_ref.at[pl.ds(k * step, step)]

    def far(d, k, owner, target):
        return pltpu.make_async_remote_copy(
            src_ref=src(k), dst_ref=spot(owner, k), send_sem=far_send.at[d - 1, k],
            recv_sem=far_recv.at[d - 1, k], device_id={"tp": target}, device_id_type=MESH)

    def near(d, k, owner, own):
        return pltpu.make_async_remote_copy(
            src_ref=src(k) if own else spot(owner, k), dst_ref=spot(owner, k),
            send_sem=near_send.at[d, k], recv_sem=near_recv.at[d, k],
            device_id={"tp": partner}, device_id_type=MESH)

    for k in range(pieces):
        for d in range(1, chips):
            far(d, k, me, chip_core(chip + d, core, chips)).start()
    for k in range(pieces):
        near(0, k, me, True).start()
    own = pltpu.make_async_copy(x_ref, out_ref.at[pl.ds(pl.multiple_of(me * rows, rows), rows)], own_sem)
    own.start()
    for k in range(pieces):
        for d in range(1, chips):
            owner = chip_core(chip - d, core, chips)
            far(d, k, owner, partner).wait_recv()
            near(d, k, owner, False).start()
    own.wait()
    for k in range(pieces):
        for d in range(1, chips):
            far(d, k, me, chip_core(chip + d, core, chips)).wait_send()
        for d in range(chips):
            sent = chip_core(chip - d, core, chips)
            got = chip_core(chip - d, CORES - 1 - core, chips)
            near(d, k, sent, d == 0).wait_send()
            near(d, k, got, d == 0).wait_recv()


def tp_gather(x, n, cid):
    rows, width = x.shape
    chips = n // CORES
    pieces = 4
    sent = 2 * rows * width * (n - 1)
    return pl.pallas_call(
        functools.partial(gather_kernel, n, pieces),
        out_shape=jax.ShapeDtypeStruct((rows * n, width), x.dtype),
        in_specs=[pl.BlockSpec(memory_space=pltpu.VMEM)],
        out_specs=pl.BlockSpec(memory_space=pl.ANY),
        scratch_shapes=[
            pltpu.SemaphoreType.DMA,
            pltpu.SemaphoreType.DMA((chips - 1, pieces)),
            pltpu.SemaphoreType.DMA((chips - 1, pieces)),
            pltpu.SemaphoreType.DMA((chips, pieces)),
            pltpu.SemaphoreType.DMA((chips, pieces)),
        ],
        compiler_params=pltpu.CompilerParams(collective_id=cid, has_side_effects=True),
        cost_estimate=pl.CostEstimate(flops=200_000_000, bytes_accessed=sent, transcendentals=0),
        name="tp_gather",
    )(x)


def scatter_kernel(n, pieces, p_ref, near_ref, far_ref, mine, theirs, load_sem, near_send, near_recv, far_send, far_recv):
    _, core, chip, chips, partner = place(n)
    rows = near_ref.shape[0]
    step = rows // pieces
    other = CORES - 1 - core
    greet(core, chip, chips, partner)

    def part(owner, k):
        return p_ref.at[pl.ds(pl.multiple_of(owner * rows + k * step, step), step)]

    def near(d, k):
        dst = near_ref.at[pl.ds(k * step, step)] if d == 0 else theirs.at[d - 1, pl.ds(k * step, step)]
        return pltpu.make_async_remote_copy(
            src_ref=part(chip_core(chip + d, other, chips), k), dst_ref=dst,
            send_sem=near_send.at[d, k], recv_sem=near_recv.at[d, k],
            device_id={"tp": partner}, device_id_type=MESH)

    def load(d, k):
        return pltpu.make_async_copy(
            part(chip_core(chip + d, core, chips), k), mine.at[d - 1, pl.ds(k * step, step)], load_sem.at[d - 1, k])

    def far(d, k):
        return pltpu.make_async_remote_copy(
            src_ref=mine.at[d - 1, pl.ds(k * step, step)], dst_ref=far_ref.at[d - 1, pl.ds(k * step, step)],
            send_sem=far_send.at[d - 1, k], recv_sem=far_recv.at[d - 1, k],
            device_id={"tp": chip_core(chip + d, core, chips)}, device_id_type=MESH)

    for k in range(pieces):
        for d in range(1, chips):
            near(d, k).start()
            load(d, k).start()
    for k in range(pieces):
        near(0, k).start()
    for k in range(pieces):
        for d in range(1, chips):
            near(d, k).wait_recv()
            load(d, k).wait()
            at = pl.ds(k * step, step)
            total = mine[d - 1, at].astype(jnp.float32) + theirs[d - 1, at].astype(jnp.float32)
            mine[d - 1, at] = total.astype(mine.dtype)
            far(d, k).start()
    for k in range(pieces):
        near(0, k).wait_recv()
        for d in range(chips):
            near(d, k).wait_send()
        for d in range(1, chips):
            far(d, k).wait()


def tp_scatter(part, n, cid):
    rows, width = part.shape[0] // n, part.shape[1]
    chips = n // CORES
    pieces = 4
    sent = 2 * rows * width * (n - 1)
    return pl.pallas_call(
        functools.partial(scatter_kernel, n, pieces),
        out_shape=(
            jax.ShapeDtypeStruct((rows, width), part.dtype),
            jax.ShapeDtypeStruct((chips - 1, rows, width), part.dtype),
        ),
        in_specs=[pl.BlockSpec(memory_space=pl.ANY)],
        out_specs=(pl.BlockSpec(memory_space=pl.ANY), pl.BlockSpec(memory_space=pl.ANY)),
        scratch_shapes=[
            pltpu.VMEM((chips - 1, rows, width), part.dtype),
            pltpu.VMEM((chips - 1, rows, width), part.dtype),
            pltpu.SemaphoreType.DMA((chips - 1, pieces)),
            pltpu.SemaphoreType.DMA((chips, pieces)),
            pltpu.SemaphoreType.DMA((chips, pieces)),
            pltpu.SemaphoreType.DMA((chips - 1, pieces)),
            pltpu.SemaphoreType.DMA((chips - 1, pieces)),
        ],
        compiler_params=pltpu.CompilerParams(collective_id=cid, has_side_effects=True),
        cost_estimate=pl.CostEstimate(flops=200_000_000, bytes_accessed=sent, transcendentals=0),
        name="tp_scatter",
    )(part)


def scattered_sum(part, n, rank, cid):
    rows = part.shape[0] // n
    near, far = tp_scatter(part, n, cid)
    own = lax.dynamic_slice_in_dim(part, rank * rows, rows, 0)
    total = own.astype(jnp.float32) + near.astype(jnp.float32)
    for d in range(far.shape[0]):
        total = total + far[d].astype(jnp.float32)
    return total


def stats_kernel(n, x_ref, out_ref, recv, send_sem, recv_sem):
    me = lax.axis_index("tp")
    barrier = pltpu.get_barrier_semaphore()
    for d in range(1, n):
        pl.semaphore_signal(barrier, inc=1, device_id={"tp": lax.rem(me + d, n)}, device_id_type=MESH)
    pl.semaphore_wait(barrier, n - 1)

    def send(d):
        return pltpu.make_async_remote_copy(
            src_ref=x_ref, dst_ref=recv.at[d - 1], send_sem=send_sem.at[d - 1],
            recv_sem=recv_sem.at[d - 1], device_id={"tp": lax.rem(me + d, n)}, device_id_type=MESH)

    for d in range(1, n):
        send(d).start()
    total = x_ref[...]
    for d in range(1, n):
        send(d).wait_recv()
        total = total + recv[d - 1]
    out_ref[...] = total
    for d in range(1, n):
        send(d).wait_send()


def tp_sum(x, n, cid):
    return pl.pallas_call(
        functools.partial(stats_kernel, n),
        out_shape=jax.ShapeDtypeStruct(x.shape, x.dtype),
        in_specs=[pl.BlockSpec(memory_space=pltpu.VMEM)],
        out_specs=pl.BlockSpec(memory_space=pltpu.VMEM),
        scratch_shapes=[
            pltpu.VMEM((n - 1,) + x.shape, x.dtype),
            pltpu.SemaphoreType.DMA((n - 1,)),
            pltpu.SemaphoreType.DMA((n - 1,)),
        ],
        compiler_params=pltpu.CompilerParams(collective_id=cid, has_side_effects=True),
        cost_estimate=pl.CostEstimate(flops=20_000_000, bytes_accessed=4 * x.size * n, transcendentals=0),
        name="tp_sum",
    )(x)


def shards(
    resid,
    norm1_gain,
    w_value,
    w_gate,
    value_scale,
    gate_scale,
    conv_taps,
    conv_gain,
    w_point,
    point_scale,
    norm2_gain,
    w_up,
    up_scale,
    w_down,
    down_scale,
):
    tok_rows = resid.shape[0]
    n = lax.axis_size("tp")
    rank = lax.axis_index("tp")
    seq_len = tok_rows * n
    channels = value_scale.shape[0]
    group_width = channels // GROUPS
    reach = conv_taps.shape[0] // 2
    own_width = w_value.shape[1]
    first_bf = jnp.concatenate(
        [w_value.astype(jnp.bfloat16), w_gate.astype(jnp.bfloat16), (w_point * point_scale).T.astype(jnp.bfloat16)],
        axis=1,
    )
    first_rows = lax.all_gather(first_bf, "fs", axis=0, tiled=True)
    up_cols = lax.all_gather(w_up.astype(jnp.bfloat16), "fs", axis=0, tiled=True)
    down_part = lax.all_gather((w_down * down_scale).astype(jnp.bfloat16), "fs", axis=1, tiled=True)
    first = rank * own_width
    own_value_scale = lax.dynamic_slice_in_dim(value_scale, first, own_width, 0)
    own_gate_scale = lax.dynamic_slice_in_dim(gate_scale, first, own_width, 0)
    own_taps = lax.dynamic_slice_in_dim(conv_taps, first, own_width, 1)
    own_gain = lax.dynamic_slice_in_dim(conv_gain, first, own_width, 0)
    normed = rms_scaled(resid, norm1_gain).astype(jnp.bfloat16)
    piece = tp_gather(normed, n, 1)
    value = jnp.dot(piece, first_rows[:, :own_width], preferred_element_type=jnp.float32) * own_value_scale
    gate = (
        jnp.dot(piece, first_rows[:, own_width : 2 * own_width], preferred_element_type=jnp.float32)
        * own_gate_scale
    )
    glu_seq = (value * jax.nn.sigmoid(gate)).astype(jnp.bfloat16)
    padded = jnp.pad(glu_seq, ((reach, reach), (0, 0)))
    conv = depthwise(padded, own_taps, seq_len)
    member = ((first + jnp.arange(own_width)) % GROUPS)[None, :] == jnp.arange(GROUPS)[:, None]
    member = member.astype(jnp.float32)
    flip = (((1,), (1,)), ((), ()))
    sums = lax.dot_general(member, conv, flip, precision=lax.Precision.HIGHEST)
    squares = lax.dot_general(member, conv * conv, flip, precision=lax.Precision.HIGHEST)
    totals = tp_sum(jnp.concatenate([sums, squares], axis=0), n, 2)
    spread = (((0,), (0,)), ((), ()))
    gmean = lax.dot_general(totals[:GROUPS] / group_width, member, spread, precision=lax.Precision.HIGHEST)
    gsquare = lax.dot_general(totals[GROUPS:] / group_width, member, spread, precision=lax.Precision.HIGHEST)
    scaled = (conv - gmean) * lax.rsqrt(gsquare - gmean * gmean + 1e-05) * own_gain
    act = jax.nn.silu(scaled).astype(jnp.bfloat16)
    mixed_part = lax.dot_general(
        act, first_rows[:, 2 * own_width :], flip, preferred_element_type=jnp.float32
    ).astype(jnp.bfloat16)
    mixed = scattered_sum(mixed_part, n, rank, 3)
    middle = (resid.astype(jnp.float32) + mixed).astype(jnp.bfloat16)
    normed2 = rms_scaled(middle, norm2_gain).astype(jnp.bfloat16)
    tokens = tp_gather(normed2, n, 4)
    upper = jnp.dot(tokens, up_cols, preferred_element_type=jnp.float32) * up_scale
    hidden = lax.optimization_barrier(jnp.square(jax.nn.relu(upper)).astype(jnp.bfloat16))
    partial = jnp.dot(hidden, down_part, preferred_element_type=jnp.float32).astype(jnp.bfloat16)
    total = scattered_sum(partial, n, rank, 5)
    return (middle.astype(jnp.float32) + total).astype(jnp.bfloat16)


def solution(mesh):
    in_specs = (
        P(("fs", "tp"), None),
        P(),
        P("fs", "tp"),
        P("fs", "tp"),
        P(),
        P(),
        P(),
        P(),
        P("tp", "fs"),
        P("fs"),
        P(),
        P("fs", "tp"),
        P("tp"),
        P("tp", "fs"),
        P("fs"),
    )
    out_specs = P(("fs", "tp"), None)
    return jax.shard_map(shards, mesh=mesh, in_specs=in_specs, out_specs=out_specs, check_vma=False)
```

time: 734 us -> 433 us (0.59)
  waiting for transfers between devices: 532 us -> 149 us
  Pallas kernels: 0 us -> 166 us
  blocking collectives: 77.1 us -> 0 us
    all_gather x7 -> x3, waiting for transfers between devices: 381 us -> 149 us  [the longest x1 99.2 us: shards(): lax.all_gather((w_down * down_scale).astype(jnp.bfloat16), 'fs', axis=1,...]
    pallas_call x0 -> x5, Pallas kernels: none -> 166 us  [the longest x2 81.4 us: tp_gather(): pl.pallas_call(functools.partial(gather_kernel, n, pieces), out_shape=jax...]
    reduce_scatter x2 -> x0, waiting for transfers between devices: 151 us -> none  [the longest x1 91.7 us: shards(): lax.psum_scatter(jnp.dot(act, point_rows, preferred_element_type=jnp.floa...]
    all_gather x2 -> x0, blocking collectives: 43.6 us -> none  [the longest x1 22.4 us: shards(): lax.all_gather(point_scale, 'fs', axis=0, tiled=True)]
    psum x1 -> x0, blocking collectives: 33.5 us -> none  [shards(): totals, square_totals = lax.psum((sums, squares), 'tp')]
    dot_general x8 -> x9, matrix products: 73 us -> 66.1 us  [the longest x1 20 us: shards(): jnp.dot(tokens, up_cols, preferred_element_type=jnp.float32) * up_scale]
  transfers between devices with their start and end apart: 9 -> 3, of which waited for: 8 -> 2; matrix products, arithmetic and copies ran while one was open for 8% -> 18% of each run, Pallas kernels for 0% -> 29%
where the time goes in v1:
time: 433 us
  Pallas kernels  166 us (38%)
  waiting for transfers between devices  149 us (34%)
  matrix products  66.1 us (15%)
  other arithmetic  31.1 us (7%)
  between operations  13.4 us (3%)
  local copies, waits for them, and re-layouts  7.3 us (2%)
    all_gather x1, waiting for transfers between devices, shards(): lax.all_gather((w_down * down_scale).astype(jnp.bfloat16), 'fs', axis=1,...  99.2 us
    pallas_call x2, Pallas kernels, tp_gather(): pl.pallas_call(functools.partial(gather_kernel, n, pieces), out_shape=jax...  81.4 us
    pallas_call x2, Pallas kernels, tp_scatter(): pl.pallas_call(functools.partial(scatter_kernel, n, pieces), out_shape=(j...  78.1 us
    all_gather x1, waiting for transfers between devices, shards(): first_rows = lax.all_gather(first_bf, 'fs', axis=0, tiled=True)  49.8 us
    dot_general x1, matrix products, shards(): jnp.dot(tokens, up_cols, preferred_element_type=jnp.float32) * up_scale  20 us
    dot_general x1, matrix products, shards(): jnp.dot(hidden, down_part, preferred_element_type=jnp.float32)  18.9 us
    add x1, other arithmetic, depthwise(): conv = conv + taps[offset] * wide[offset:offset + length]  12.2 us
  transfers between devices with their start and end apart: 3, of which 2 were waited for; matrix products, arithmetic and copies ran while one was open for 18% of the time, Pallas kernels for 29%

profile of v1, /device:TPU:0, one launch (start us, length us, event | category | flops | bytes accessed | tf_op | source)
XLA Modules:
  0.0 432.6 jit_solution(14628866819288935875)
XLA Ops:
  6.5 1.3 copy.16
  7.9 1.2 copy.17
  9.0 1.1 fusion.53
  10.1 1.0 pad_maximum_fusion
  11.2 1.1 convert_element_type.100
  12.4 2.9 multiply_convert_fusion.2
  15.7 0.8 dynamic_slice.20
  16.5 0.8 dynamic_slice.19
  17.3 0.8 dynamic_slice.21
  18.0 1.6 fusion.11.x_ref
  19.6 41.6 %tp_gather.2 = bf16[1536,2048]{1,0:T(8,128)(2,1)} custom-call(bf16[384,2048]{1,0:T(8,128)(2,1)} %fusion.11.x_ref), custom_call_target="tpu_custom_call" | custom-call | flops 200000000 | bytes 4718592 | tf_op jit(solution)/shard_map/tp_gather/pallas_call | solution.py:103
  61.2 1.2 fusion.70
  62.5 1.2 constant_dynamic-slice_fusion
  63.7 49.8 %all-gather.4.cloned.1.call-done = bf16[2048,1536]{0,1:T(8,128)(2,1)} async-done(((bf16[256,1536]{0,1:T(8,128)(2,1)}), bf16[2048,1536]{0,1:T(8,128)(2,1)}) %all-gather.4.cloned.1.call-update) | async-done | bytes 6291472 | tf_op jit(solution)/shard_map/all_gather | solution.py:277
  113.5 6.8 %fusion.8 = f32[1536,512]{1,0:T(8,128)S(1)} fusion(bf16[1536,2048]{1,0:T(8,128)(2,1)} %tp_gather.2, bf16[2048,1536]{0,1:T(8,128)(2,1)} %all-gather.4.cloned.1.call-done, f32[512]{0:T(512)S(1)} %dynamic_slice.20), kind=kOutput, calls=%fused_computation.20 | convolution fusion | flops 3224371200 | bytes 11536384 | tf_op jit(solution)/shard_map/dot_general | solution.py:289
  120.3 5.4 %fusion.49 = bf16[1536,512]{1,0:T(8,128)(2,1)S(1)} fusion(f32[1536,512]{1,0:T(8,128)S(1)} %fusion.8, bf16[1536,2048]{1,0:T(8,128)(2,1)S(1)} %copy-done.2, bf16[2048,1536]{0,1:T(8,128)(2,1)} %all-gather.4.cloned.1.call-done, f32[512]{0:T(512)S(1)} %dynamic_slice.19), kind=kOutput, calls=%fused_computation.95 | convolution fusion | flops 3223584768 | bytes 13109248 | tf_op jit(solution)/shard_map/dot_general | solution.py:287
  126.2 12.2 %fusion.17 = f32[1536,512]{1,0:T(8,128)S(1)} fusion(f32[1566,512]{1,0:T(8,128)S(1)} %pad_convert_fusion, f32[512]{0:T(512)S(1)} %bitcast.60, f32[512]{0:T(512)S(1)} %bitcast.62, f32[512]{0:T(512)S(1)} %bitcast.63, f32[512]{0:T(512)S(1)} %bitcast.64, f32[512]{0:T(512)S(1)} %bitcast.65, f32[512]{0:T(512)S(1)} %bitcast.66, f32[512]{0:T(512)S(1)} %bitcast.67, ...), kind=kLoop, calls=%fused_computation.30 | loop fusion | flops 47972352 | bytes 100726784 | tf_op jit(solution)/shard_map/add | solution.py:25
  138.4 1.5 fusion.61
  139.9 1.6 fusion.47
  142.1 6.0 %tp_sum.1 = f32[8,1536]{1,0:T(8,128)} custom-call(f32[8,1536]{1,0:T(8,128)} %pad_maximum_fusion.1.x_ref), custom_call_target="tpu_custom_call" | custom-call | flops 20000000 | bytes 196608 | tf_op jit(solution)/shard_map/tp_sum/pallas_call | solution.py:232
  148.2 2.3 fusion.56
  150.5 2.7 multiply_convert_fusion.1
  153.3 6.9 %convolution_convert_fusion.1.p_ref = bf16[1536,2048]{1,0:T(8,128)(2,1)} fusion(bf16[1536,512]{1,0:T(8,128)(2,1)S(1)} %multiply_convert_fusion.1, bf16[2048,1536]{0,1:T(8,128)(2,1)} %all-gather.4.cloned.1.call-done), kind=kOutput, calls=%fused_computation.2 | convolution fusion | flops 3224371200 | bytes 9961472 | tf_op jit(solution)/shard_map/dot_general | solution.py:306
  160.2 39.2 %tp_scatter.2 = (bf16[384,2048]{1,0:T(8,128)(2,1)}, bf16[1,384,2048]{2,1,0:T(8,128)(2,1)}) custom-call(bf16[1536,2048]{1,0:T(8,128)(2,1)} %convolution_convert_fusion.1.p_ref), custom_call_target="tpu_custom_call" | custom-call | flops 200000000 | bytes 4718592 | tf_op jit(solution)/shard_map/tp_scatter/pallas_call | solution.py:175
  199.4 3.5 fusion.13
  202.9 1.6 fusion.15.x_ref
  204.5 39.8 %tp_gather.3 = bf16[1536,2048]{1,0:T(8,128)(2,1)} custom-call(bf16[384,2048]{1,0:T(8,128)(2,1)} %fusion.15.x_ref), custom_call_target="tpu_custom_call" | custom-call | flops 200000000 | bytes 4718592 | tf_op jit(solution)/shard_map/tp_gather/pallas_call | solution.py:103
  244.3 20.0 %multiply_convert_fusion = bf16[1536,2048]{1,0:T(8,128)(2,1)} fusion(bf16[1536,2048]{1,0:T(8,128)(2,1)} %tp_gather.3, bf16[2048,2048]{1,0:T(8,128)(2,1)} %all-gather.6.cloned.1.call-done, f32[2048]{0:T(1024)S(1)} %copy-done.8), kind=kOutput, calls=%fused_computation | convolution fusion | flops 12897484800 | bytes 20979712 | tf_op jit(solution)/shard_map/dot_general | solution.py:313
  264.3 99.2 %all-gather.8.cloned.1.call-done = bf16[2048,2048]{1,0:T(8,128)(2,1)} async-done(((bf16[2048,256]{1,0:T(8,128)(2,1)}), bf16[2048,2048]{1,0:T(8,128)(2,1)}) %all-gather.8.cloned.1.call-update) | async-done | bytes 8388624 | tf_op jit(solution)/shard_map/all_gather | solution.py:279
  363.5 18.9 %convolution_convert_fusion.p_ref = bf16[1536,2048]{1,0:T(8,128)(2,1)} fusion(bf16[1536,2048]{1,0:T(8,128)(2,1)} %multiply_convert_fusion, bf16[2048,2048]{1,0:T(8,128)(2,1)} %all-gather.8.cloned.1.call-done), kind=kOutput, calls=%fused_computation.1 | convolution fusion | flops 12888047616 | bytes 20971520 | tf_op jit(solution)/shard_map/dot_general | solution.py:315
  382.4 39.0 %tp_scatter.3 = (bf16[384,2048]{1,0:T(8,128)(2,1)}, bf16[1,384,2048]{2,1,0:T(8,128)(2,1)}) custom-call(bf16[1536,2048]{1,0:T(8,128)(2,1)} %convolution_convert_fusion.p_ref), custom_call_target="tpu_custom_call" | custom-call | flops 200000000 | bytes 4718592 | tf_op jit(solution)/shard_map/tp_scatter/pallas_call | solution.py:175
  421.3 4.7 %fusion.16 = bf16[384,2048]{1,0:T(8,128)(2,1)} fusion(bf16[384,2048]{1,0:T(8,128)(2,1)S(1)} %get-tuple-element.14, bf16[384,2048]{1,0:T(8,128)(2,1)} %get-tuple-element.11, bf16[1,384,2048]{2,1,0:T(8,128)(2,1)} %get-tuple-element.12, bf16[1536,2048]{1,0:T(8,128)(2,1)} %convolution_convert_fusion.p_ref, s32[]{:T(128)S(6)} %select_n.23), kind=kLoop, calls=%fused_computation.28 | loop fusion | flops 6291456 | bytes 7864324 | tf_op jit(solution)/shard_map/convert_element_type | solution.py:317
  (31 shorter events, 1.7 us)
Async XLA Ops:
  6.5 4.6 %copy-start.3 = (f32[256,2048]{1,0:T(8,128)S(1)}, f32[256,2048]{1,0:T(8,128)}, u32[]{:S(2)}) copy-start(f32[256,2048]{1,0:T(8,128)} %param.26) | copy-start | bytes 6291460
  6.5 106.9 %all-gather.4.cloned.1.call-start = ((), (), s32[]{:S(2)}) async-start(), calls=%async_computation | async-start | bytes 7077888 | tf_op jit(solution)/shard_map/all_gather | solution.py:277
  10.1 2.2 copy-start.7
  11.1 233.2 %all-gather.6.cloned.1.call-start = ((), (), s32[]{:S(2)}) async-start(), calls=%async_computation.1 | async-start | bytes 9437184 | tf_op jit(solution)/shard_map/all_gather | solution.py:278
  12.3 3.0 copy-start
  12.3 5.7 %copy-start.5 = (f32[2048]{0:T(1024)S(1)}, f32[2048]{0:T(1024)}, u32[]{:S(2)}) copy-start(f32[2048]{0:T(1024)} %param.16) | copy-start | bytes 24580
  12.3 351.2 %all-gather.8.cloned.1.call-start = ((), (), s32[]{:S(2)}) async-start(), calls=%async_computation.2 | async-start | bytes 9437184 | tf_op jit(solution)/shard_map/all_gather | solution.py:279
  113.5 6.8 %copy-start.2 = (bf16[1536,2048]{1,0:T(8,128)(2,1)S(1)}, bf16[1536,2048]{1,0:T(8,128)(2,1)}, u32[]{:S(2)}) copy-start(bf16[1536,2048]{1,0:T(8,128)(2,1)} %tp_gather.2) | copy-start | bytes 18874372
  148.2 2.3 copy-start.4
  160.2 39.2 %copy-start.1 = (bf16[384,2048]{1,0:T(8,128)(2,1)S(1)}, bf16[384,2048]{1,0:T(8,128)(2,1)}, u32[]{:S(2)}) copy-start(bf16[384,2048]{1,0:T(8,128)(2,1)} %param.15) | copy-start | bytes 4718596
  199.4 3.5 copy-start.6
  204.5 39.8 %copy-start.8 = (f32[2048]{0:T(1024)S(1)}, f32[2048]{0:T(1024)}, u32[]{:S(2)}) copy-start(f32[2048]{0:T(1024)} %param.27) | copy-start | bytes 24580
Sparse Core Ops, SparseCore 0:
  11.2 102.1 all-gather.3
  115.6 122.6 all-gather.5
  240.3 123.1 all-gather.7

commit v2 on v1

--- a/solution.py
+++ b/solution.py
@@ -243,6 +243,180 @@
         cost_estimate=pl.CostEstimate(flops=20_000_000, bytes_accessed=4 * x.size * n, transcendentals=0),
         name="tp_sum",
     )(x)
+
+
+def ring_at(q, count):
+    q = lax.rem(q + 2 * count, count)
+    high = q // (count // 2)
+    return (1 - high) * 2 * q + high * (2 * (count - 1 - q) + 1)
+
+
+def mlp_kernel(
+    n, count, tok_ref, up_ref, scale_ref, w_ref, mid_ref, out_ref,
+    hidden, held, part, theirs, near_in, far_in,
+    cw_send, cw_recv, ccw_send, ccw_recv, near_send, near_recv, far_send, far_recv,
+):
+    me, core, chip, chips, partner = place(n)
+    seat = lax.axis_index("fs")
+    odd = lax.rem(seat, 2)
+    pos = (1 - odd) * (seat // 2) + odd * (count - 1 - seat // 2)
+    right, left = ring_at(pos + 1, count), ring_at(pos - 1, count)
+    rows, width = mid_ref.shape[0], w_ref.shape[1]
+    depth = w_ref.shape[0]
+    half = depth // 2
+    far_step = count // 2
+    other = CORES - 1 - core
+    tile = 256
+
+    barrier = pltpu.get_barrier_semaphore()
+    for target in (left, right):
+        pl.semaphore_signal(barrier, inc=1, device_id={"fs": target}, device_id_type=MESH)
+    pl.semaphore_signal(barrier, inc=1, device_id={"tp": partner}, device_id_type=MESH)
+    for d in range(1, chips):
+        pl.semaphore_signal(
+            barrier, inc=1, device_id={"tp": chip_core(chip + d, core, chips)}, device_id_type=MESH
+        )
+    pl.semaphore_wait(barrier, chips + 2)
+
+    def hop(s, k, clockwise):
+        at = pl.ds(k * half, half)
+        before = s - 1 if clockwise else count - s + 1
+        after = s if clockwise else count - s
+        src = w_ref.at[at] if s == 1 else held.at[before, at]
+        return pltpu.make_async_remote_copy(
+            src_ref=src, dst_ref=held.at[after, at],
+            send_sem=(cw_send if clockwise else ccw_send).at[s - 1, k],
+            recv_sem=(cw_recv if clockwise else ccw_recv).at[s - 1, k],
+            device_id={"fs": right if clockwise else left}, device_id_type=MESH)
+
+    def carries(s, k, clockwise):
+        return s < far_step or (s == far_step and k == (0 if clockwise else 1))
+
+    def pass_on(s, k):
+        for clockwise in (True, False):
+            if carries(s, k, clockwise):
+                hop(s, k, clockwise).wait_recv()
+                if carries(s + 1, k, clockwise):
+                    hop(s + 1, k, clockwise).start()
+
+    def expand(piece, pieces):
+        span = up_ref.shape[1] // pieces
+        block = min(512, span)
+
+        @pl.loop(0, tok_ref.shape[0] // tile)
+        def _(t):
+            at = pl.ds(pl.multiple_of(t * tile, tile), tile)
+            for c in range(piece * span, (piece + 1) * span, block):
+                upper = jnp.dot(tok_ref[at, :], up_ref[:, c : c + block], preferred_element_type=jnp.float32)
+                upper = jnp.maximum(upper * scale_ref[:, c : c + block], 0.0)
+                hidden[at, c : c + block] = (upper * upper).astype(hidden.dtype)
+
+    def rows_of(owner):
+        return pl.ds(pl.multiple_of(owner * rows, rows), rows)
+
+    def near(j, d):
+        return pltpu.make_async_remote_copy(
+            src_ref=part.at[j, rows_of(chip_core(chip + d, other, chips))],
+            dst_ref=near_in.at[j] if d == 0 else theirs.at[j, d - 1],
+            send_sem=near_send.at[j, d], recv_sem=near_recv.at[j, d],
+            device_id={"tp": partner}, device_id_type=MESH)
+
+    def far(j, d):
+        return pltpu.make_async_remote_copy(
+            src_ref=part.at[j, rows_of(chip_core(chip + d, core, chips))], dst_ref=far_in.at[j, d - 1],
+            send_sem=far_send.at[j, d - 1], recv_sem=far_recv.at[j, d - 1],
+            device_id={"tp": chip_core(chip + d, core, chips)}, device_id_type=MESH)
+
+    def contract(j):
+        @pl.loop(0, tok_ref.shape[0] // tile)
+        def _(t):
+            at = pl.ds(pl.multiple_of(t * tile, tile), tile)
+            weight = w_ref[...] if j == 0 else held[j]
+            part[j, at, :] = jnp.dot(hidden[at, :], weight, preferred_element_type=jnp.float32).astype(part.dtype)
+
+        for d in list(range(1, chips)) + [0]:
+            near(j, d).start()
+
+    def combine(j):
+        for d in range(1, chips):
+            near(j, d).wait_recv()
+            at = rows_of(chip_core(chip + d, core, chips))
+            total = part[j, at, :].astype(jnp.float32) + theirs[j, d - 1].astype(jnp.float32)
+            part[j, at, :] = total.astype(part.dtype)
+            far(j, d).start()
+
+    def finish(j):
+        near(j, 0).wait_recv()
+        total = part[j, rows_of(me), :].astype(jnp.float32) + near_in[j].astype(jnp.float32)
+        for d in range(1, chips):
+            far(j, d).wait_recv()
+            total = total + far_in[j, d - 1].astype(jnp.float32)
+        at = pl.ds(pl.multiple_of(ring_at(pos - j, count) * width, width), width)
+        out_ref[:, at] = (mid_ref[:, at].astype(jnp.float32) + total).astype(out_ref.dtype)
+
+    for k in range(2):
+        for clockwise in (True, False):
+            if carries(1, k, clockwise):
+                hop(1, k, clockwise).start()
+    expand(0, 2)
+    pass_on(1, 0)
+    expand(1, 2)
+    pass_on(1, 1)
+    groups = [[0]] + [[s, count - s] if s < far_step else [s] for s in range(1, far_step + 1)]
+    for s, group in enumerate(groups):
+        if s > 1:
+            pass_on(s, 0)
+            pass_on(s, 1)
+        for j in group:
+            contract(j)
+        for j in group:
+            combine(j)
+        if s > 1:
+            for j in groups[s - 2]:
+                finish(j)
+    for group in groups[-2:]:
+        for j in group:
+            finish(j)
+    for s in range(1, far_step + 1):
+        for k in range(2):
+            for clockwise in (True, False):
+                if carries(s, k, clockwise):
+                    hop(s, k, clockwise).wait_send()
+    for j in range(count):
+        for d in range(chips):
+            near(j, d).wait_send()
+        for d in range(1, chips):
+            far(j, d).wait_send()
+
+
+def ring_mlp(tokens, up_cols, up_scale, down, middle, n, count, cid):
+    seq, rows = tokens.shape[0], middle.shape[0]
+    depth, width = down.shape
+    chips = n // CORES
+    kind = tokens.dtype
+    steps = count // 2
+    dma = pltpu.SemaphoreType.DMA
+    return pl.pallas_call(
+        functools.partial(mlp_kernel, n, count),
+        out_shape=jax.ShapeDtypeStruct(middle.shape, middle.dtype),
+        in_specs=[pl.BlockSpec(memory_space=pltpu.VMEM)] * 5,
+        out_specs=pl.BlockSpec(memory_space=pltpu.VMEM),
+        scratch_shapes=[
+            pltpu.VMEM((seq, depth), kind),
+            pltpu.VMEM((count, depth, width), kind),
+            pltpu.VMEM((count, seq, width), kind),
+            pltpu.VMEM((count, chips - 1, rows, width), kind),
+            pltpu.VMEM((count, rows, width), kind),
+            pltpu.VMEM((count, chips - 1, rows, width), kind),
+            dma((steps, 2)), dma((steps, 2)), dma((steps, 2)), dma((steps, 2)),
+            dma((count, chips)), dma((count, chips)), dma((count, chips - 1)), dma((count, chips - 1)),
+        ],
+        compiler_params=pltpu.CompilerParams(
+            collective_id=cid, has_side_effects=True, vmem_limit_bytes=60 * 1024 * 1024
+        ),
+        cost_estimate=pl.CostEstimate(flops=4 * seq * depth * width * count, bytes_accessed=4 * seq * depth, transcendentals=0),
+        name="ring_mlp",
+    )(tokens, up_cols, up_scale.reshape(1, -1), down, middle)
 
 
 def shards(
@@ -276,7 +450,7 @@
     )
     first_rows = lax.all_gather(first_bf, "fs", axis=0, tiled=True)
     up_cols = lax.all_gather(w_up.astype(jnp.bfloat16), "fs", axis=0, tiled=True)
-    down_part = lax.all_gather((w_down * down_scale).astype(jnp.bfloat16), "fs", axis=1, tiled=True)
+    down_bf = (w_down * down_scale).astype(jnp.bfloat16)
     first = rank * own_width
     own_value_scale = lax.dynamic_slice_in_dim(value_scale, first, own_width, 0)
     own_gate_scale = lax.dynamic_slice_in_dim(gate_scale, first, own_width, 0)
@@ -310,11 +484,7 @@
     middle = (resid.astype(jnp.float32) + mixed).astype(jnp.bfloat16)
     normed2 = rms_scaled(middle, norm2_gain).astype(jnp.bfloat16)
     tokens = tp_gather(normed2, n, 4)
-    upper = jnp.dot(tokens, up_cols, preferred_element_type=jnp.float32) * up_scale
-    hidden = lax.optimization_barrier(jnp.square(jax.nn.relu(upper)).astype(jnp.bfloat16))
-    partial = jnp.dot(hidden, down_part, preferred_element_type=jnp.float32).astype(jnp.bfloat16)
-    total = scattered_sum(partial, n, rank, 5)
-    return (middle.astype(jnp.float32) + total).astype(jnp.bfloat16)
+    return ring_mlp(tokens, up_cols, up_scale, down_bf, middle, n, lax.axis_size("fs"), 5)
 
 
 def solution(mesh):

time: 433 us -> 354 us (0.82)
  waiting for transfers between devices: 149 us -> 50 us
  Pallas kernels: 166 us -> 226 us
  matrix products: 66.1 us -> 27.2 us
  other arithmetic: 31.1 us -> 26.3 us
    pallas_call x0 -> x1, Pallas kernels: none -> 99.8 us  [ring_mlp(): pl.pallas_call(functools.partial(mlp_kernel, n, count), out_shape=jax.Sha...]
    all_gather x1 -> x0, waiting for transfers between devices: 99.2 us -> none  [shards(): lax.all_gather((w_down * down_scale).astype(jnp.bfloat16), 'fs', axis=1,...]
    pallas_call x2 -> x1, Pallas kernels: 78.1 us -> 39.2 us  [tp_scatter(): pl.pallas_call(functools.partial(scatter_kernel, n, pieces), out_shape=(j...]
    dot_general x2 -> x0, matrix products: 38.9 us -> none  [the longest x1 20 us: shards(): jnp.dot(tokens, up_cols, preferred_element_type=jnp.float32) * up_scale]
    convert_element_type x2 -> x1, other arithmetic: 7.61 us -> 1.17 us  [shards(): down_bf = (w_down * down_scale).astype(jnp.bfloat16)]
  transfers between devices with their start and end apart: 3 -> 2, of which waited for: 2 -> 1; matrix products, arithmetic and copies ran while one was open for 18% -> 16% of each run, Pallas kernels for 29% -> 36%
where the time goes in v2:
time: 354 us
  Pallas kernels  226 us (64%)
  waiting for transfers between devices  50 us (14%)
  matrix products  27.2 us (8%)
  other arithmetic  26.3 us (7%)
  between operations  13.7 us (4%)
  local copies, waits for them, and re-layouts  9.89 us (3%)
    pallas_call x1, Pallas kernels, ring_mlp(): pl.pallas_call(functools.partial(mlp_kernel, n, count), out_shape=jax.Sha...  99.8 us
    pallas_call x2, Pallas kernels, tp_gather(): pl.pallas_call(functools.partial(gather_kernel, n, pieces), out_shape=jax...  81.4 us
    all_gather x1, waiting for transfers between devices, shards(): first_rows = lax.all_gather(first_bf, 'fs', axis=0, tiled=True)  50 us
    pallas_call x1, Pallas kernels, tp_scatter(): pl.pallas_call(functools.partial(scatter_kernel, n, pieces), out_shape=(j...  39.2 us
    add x1, other arithmetic, depthwise(): conv = conv + taps[offset] * wide[offset:offset + length]  12.2 us
  transfers between devices with their start and end apart: 2, of which 1 were waited for; matrix products, arithmetic and copies ran while one was open for 16% of the time, Pallas kernels for 36%

profile of v2, /device:TPU:0, one launch (start us, length us, event | category | flops | bytes accessed | tf_op | source)
XLA Modules:
  0.0 353.5 jit_solution(4749123245545215237)
XLA Ops:
  6.5 1.2 copy.16
  7.7 1.2 copy.17
  8.9 1.1 fusion.52
  10.0 0.9 pad_maximum_fusion
  11.0 2.7 convert_element_type.78
  13.8 0.8 dynamic_slice.17
  14.5 0.8 dynamic_slice.16
  15.3 0.8 dynamic_slice.18
  16.1 0.4 fusion.12
  16.5 1.6 fusion.14.x_ref
  18.0 41.6 %tp_gather.2 = bf16[1536,2048]{1,0:T(8,128)(2,1)} custom-call(bf16[384,2048]{1,0:T(8,128)(2,1)} %fusion.14.x_ref), custom_call_target="tpu_custom_call" | custom-call | flops 200000000 | bytes 4718592 | tf_op jit(solution)/shard_map/tp_gather/pallas_call | solution.py:103
  59.7 1.2 fusion.69
  60.9 1.3 constant_dynamic-slice_fusion
  62.2 1.2 multiply_convert_fusion.1.w_ref
  63.4 50.0 %all-gather.3.cloned.1.call-done = bf16[2048,1536]{0,1:T(8,128)(2,1)} async-done(((bf16[256,1536]{0,1:T(8,128)(2,1)}), bf16[2048,1536]{0,1:T(8,128)(2,1)}) %all-gather.3.cloned.1.call-update) | async-done | bytes 6291472 | tf_op jit(solution)/shard_map/all_gather | solution.py:451
  113.3 6.8 %fusion.8 = f32[1536,512]{1,0:T(8,128)S(1)} fusion(bf16[1536,2048]{1,0:T(8,128)(2,1)} %tp_gather.2, bf16[2048,1536]{0,1:T(8,128)(2,1)} %all-gather.3.cloned.1.call-done, f32[512]{0:T(512)S(1)} %dynamic_slice.17), kind=kOutput, calls=%fused_computation.17 | convolution fusion | flops 3224371200 | bytes 11536384 | tf_op jit(solution)/shard_map/dot_general | solution.py:463
  120.1 5.4 %fusion.48 = bf16[1536,512]{1,0:T(8,128)(2,1)S(1)} fusion(f32[1536,512]{1,0:T(8,128)S(1)} %fusion.8, bf16[1536,2048]{1,0:T(8,128)(2,1)S(1)} %copy-done.2, bf16[2048,1536]{0,1:T(8,128)(2,1)} %all-gather.3.cloned.1.call-done, f32[512]{0:T(512)S(1)} %dynamic_slice.16), kind=kOutput, calls=%fused_computation.90 | convolution fusion | flops 3223584768 | bytes 13109248 | tf_op jit(solution)/shard_map/dot_general | solution.py:461
  125.6 0.5 pad_convert_fusion
  126.0 12.2 %fusion.16 = f32[1536,512]{1,0:T(8,128)S(1)} fusion(f32[1566,512]{1,0:T(8,128)S(1)} %pad_convert_fusion, f32[512]{0:T(512)S(1)} %bitcast.54, f32[512]{0:T(512)S(1)} %bitcast.56, f32[512]{0:T(512)S(1)} %bitcast.57, f32[512]{0:T(512)S(1)} %bitcast.58, f32[512]{0:T(512)S(1)} %bitcast.59, f32[512]{0:T(512)S(1)} %bitcast.60, f32[512]{0:T(512)S(1)} %bitcast.61, ...), kind=kLoop, calls=%fused_computation.26 | loop fusion | flops 47972352 | bytes 100726784 | tf_op jit(solution)/shard_map/add | solution.py:25
  138.2 1.5 fusion.60
  139.7 1.6 fusion.46
  141.3 0.6 pad_maximum_fusion.1.x_ref
  142.0 6.1 %tp_sum.1 = f32[8,1536]{1,0:T(8,128)} custom-call(f32[8,1536]{1,0:T(8,128)} %pad_maximum_fusion.1.x_ref), custom_call_target="tpu_custom_call" | custom-call | flops 20000000 | bytes 196608 | tf_op jit(solution)/shard_map/tp_sum/pallas_call | solution.py:232
  148.1 2.3 fusion.55
  150.4 2.7 multiply_convert_fusion
  153.1 6.8 %convolution_convert_fusion.p_ref = bf16[1536,2048]{1,0:T(8,128)(2,1)} fusion(bf16[1536,512]{1,0:T(8,128)(2,1)S(1)} %multiply_convert_fusion, bf16[2048,1536]{0,1:T(8,128)(2,1)} %all-gather.3.cloned.1.call-done), kind=kOutput, calls=%fused_computation | convolution fusion | flops 3224371200 | bytes 9961472 | tf_op jit(solution)/shard_map/dot_general | solution.py:480
  160.0 39.2 %tp_scatter.1 = (bf16[384,2048]{1,0:T(8,128)(2,1)}, bf16[1,384,2048]{2,1,0:T(8,128)(2,1)}) custom-call(bf16[1536,2048]{1,0:T(8,128)(2,1)} %convolution_convert_fusion.p_ref), custom_call_target="tpu_custom_call" | custom-call | flops 200000000 | bytes 4718592 | tf_op jit(solution)/shard_map/tp_scatter/pallas_call | solution.py:175
  199.2 3.5 fusion.9
  202.7 1.6 fusion.11.x_ref
  204.4 39.8 %tp_gather.3.tok_ref = bf16[1536,2048]{1,0:T(8,128)(2,1)} custom-call(bf16[384,2048]{1,0:T(8,128)(2,1)} %fusion.11.x_ref), custom_call_target="tpu_custom_call" | custom-call | flops 200000000 | bytes 4718592 | tf_op jit(solution)/shard_map/tp_gather/pallas_call | solution.py:103
  244.2 99.8 %ring_mlp.1 = bf16[384,2048]{1,0:T(8,128)(2,1)} custom-call(bf16[1536,2048]{1,0:T(8,128)(2,1)} %tp_gather.3.tok_ref, bf16[2048,2048]{1,0:T(8,128)(2,1)} %all-gather.5.cloned.1.call-done.up_ref, f32[1,2048]{1,0:T(1,128)} %bitcast.73, bf16[2048,256]{1,0:T(8,128)(2,1)} %multiply_convert_fusion.1.w_ref, bf16[384,2048]{1,0:T(8,128)(2,1)} %copy-done.3), custom_call_target="tpu_custom_call" | custom-call | flops 25769803776 | bytes 12582912 | tf_op jit(solution)/shard_map/ring_mlp/pallas_call | solution.py:399
  343.9 2.7 copy.19
  (26 shorter events, 0.2 us)
Async XLA Ops:
  6.5 106.8 %all-gather.3.cloned.1.call-start = ((), (), s32[]{:S(2)}) async-start(), calls=%async_computation | async-start | bytes 7077888 | tf_op jit(solution)/shard_map/all_gather | solution.py:451
  10.0 6.1 %copy-start = (bf16[384,2048]{1,0:T(8,128)(2,1)S(1)}, bf16[384,2048]{1,0:T(8,128)(2,1)}, u32[]{:S(2)}) copy-start(bf16[384,2048]{1,0:T(8,128)(2,1)} %param.15) | copy-start | bytes 4718596
  11.0 5.5 %copy-start.6 = (f32[2048]{0:T(1024)S(1)}, f32[2048]{0:T(1024)}, u32[]{:S(2)}) copy-start(f32[2048]{0:T(1024)} %param.16) | copy-start | bytes 24580
  11.0 233.2 %all-gather.5.cloned.1.call-start = ((), (), s32[]{:S(2)}) async-start(), calls=%async_computation.1 | async-start | bytes 9437184 | tf_op jit(solution)/shard_map/all_gather | solution.py:452
  18.0 44.2 %copy-start.4 = (f32[2048,256]{1,0:T(8,128)S(1)}, f32[2048,256]{1,0:T(8,128)}, u32[]{:S(2)}) copy-start(f32[2048,256]{1,0:T(8,128)} %param.28) | copy-start | bytes 6291460
  18.0 44.2 %copy-start.8 = (f32[256]{0:T(256)S(1)}, f32[256]{0:T(256)}, u32[]{:S(2)}) copy-start(f32[256]{0:T(256)} %param.29) | copy-start | bytes 3076
  113.3 6.8 %copy-start.2 = (bf16[1536,2048]{1,0:T(8,128)(2,1)S(1)}, bf16[1536,2048]{1,0:T(8,128)(2,1)}, u32[]{:S(2)}) copy-start(bf16[1536,2048]{1,0:T(8,128)(2,1)} %tp_gather.2) | copy-start | bytes 18874372
  148.1 2.3 copy-start.5
  160.0 39.2 %copy-start.1 = (bf16[384,2048]{1,0:T(8,128)(2,1)S(1)}, bf16[384,2048]{1,0:T(8,128)(2,1)}, u32[]{:S(2)}) copy-start(bf16[384,2048]{1,0:T(8,128)(2,1)} %param.15) | copy-start | bytes 4718596
  199.2 3.5 %copy-start.7 = (f32[2048]{0:T(1024)S(1)}, f32[2048]{0:T(1024)}, u32[]{:S(2)}) copy-start(f32[2048]{0:T(1024)} %param.25) | copy-start | bytes 24580
  202.7 41.4 %copy-start.3 = (bf16[384,2048]{1,0:T(8,128)(2,1)}, bf16[384,2048]{1,0:T(8,128)(2,1)S(1)}, u32[]{:S(2)}) copy-start(bf16[384,2048]{1,0:T(8,128)(2,1)S(1)} %get-tuple-element.10.mid_ref) | copy-start | bytes 4718596
Sparse Core Ops, SparseCore 0:
  11.1 102.1 all-gather.2
  115.4 122.6 all-gather.4
